TPU v7x, 32 devices: a whole 2x2x4 slice. The times are simulated.
32 devices in a mesh: ep: 4 (over y, x), tp: 8 (over z, core).
Axes of the slice: x: 2, y: 2, z: 4, core: 2. Of those that a mesh axis runs over, the one named last changes fastest.
Arguments:
- tokens: bfloat16 [896, 4096], P('ep', 'tp'), may hold values from -6 to 6
- picks: int32 [4, 4, 56], P('ep'), may hold values from 0 to 223, as said below
- pick_weights: float32 [4, 4, 56], P('ep'), may hold values from 0.1 to 1
- gate_weight: bfloat16 [4, 1280, 4096], P('ep', 'tp'), may hold values from -0.09375 to 0.09375
- up_weight: bfloat16 [4, 1280, 4096], P('ep', 'tp'), may hold values from -0.09375 to 0.09375
- down_weight: bfloat16 [4, 1280, 4096], P('ep', None, 'tp'), may hold values from -0.15625 to 0.15625
- dense_gate: bfloat16 [5120, 4096], P('tp'), may hold values from -0.09375 to 0.09375
- dense_up: bfloat16 [5120, 4096], P('tp'), may hold values from -0.09375 to 0.09375
- dense_down: bfloat16 [5120, 4096], P('tp'), may hold values from -0.078125 to 0.078125
- branch_gate: float32 [4096], P('tp'), may hold values from -6 to 6
Outputs:
- mixed: bfloat16 [896, 4096], P('ep', 'tp')
Inputs may be any that keep to these rules, and one draw needn't show every extreme that they name: For each block s and expert e, the 56 entries picks[s, e, :] are distinct rows of that block.
All inputs are finite; a program needn't handle non-finite values.
Results may differ from a plain program's by a relative error of at most 0.014.
Values may be sent and summed in bfloat16 or wider, within the bound.
A program may use at most 64 MiB of HBM per device.

v0:
```python
import jax
import jax.numpy as jnp
from jax import lax
from jax.sharding import PartitionSpec as P


def per_device(
    tokens,
    picks,
    pick_weights,
    gate_weight,
    up_weight,
    down_weight,
    dense_gate,
    dense_up,
    dense_down,
    branch_gate,
):
    tok_rows = tokens.shape[0]
    experts = picks.shape[1]
    slots = picks.shape[2]
    chosen = picks.reshape(-1)
    full_rows = lax.all_gather(tokens, "tp", axis=1, tiled=True)
    picked = jnp.take(tokens, chosen, axis=0).reshape(experts, slots, tokens.shape[1])
    landed = lax.all_to_all(picked, "ep", split_axis=0, concat_axis=0, tiled=True)
    arrived = lax.all_gather(landed, "tp", axis=2, tiled=True)
    expert_rows = arrived.reshape(-1, arrived.shape[2])
    contract_last = (((1,), (1,)), ((), ()))
    gate_value = lax.dot_general(
        gate_weight[0], expert_rows, contract_last, preferred_element_type=jnp.float32
    )
    up_value = lax.dot_general(
        up_weight[0], expert_rows, contract_last, preferred_element_type=jnp.float32
    )
    hidden = (jax.nn.silu(gate_value) * up_value).astype(jnp.bfloat16)
    columns = down_weight[0]
    expert_out = lax.dot_general(
        lax.all_gather(hidden, "tp", axis=0, tiled=True),
        columns,
        (((0,), (0,)), ((), ())),
        preferred_element_type=jnp.float32,
    ).astype(jnp.bfloat16)
    sent_back = lax.all_to_all(
        expert_out.reshape(-1, slots, columns.shape[1]),
        "ep",
        split_axis=0,
        concat_axis=0,
        tiled=True,
    )
    row_ids = lax.broadcasted_iota(jnp.int32, (experts, tok_rows, slots), 1)
    matches = row_ids == picks[0][:, None, :]
    selector = matches.astype(jnp.bfloat16)
    token_weights = jnp.sum(jnp.where(matches, pick_weights[0][:, None, :], 0.0), axis=2)
    placed = jnp.einsum("ets,esd->etd", selector, sent_back, preferred_element_type=jnp.float32)
    mixture = jnp.sum(token_weights[:, :, None] * placed, axis=0)
    dense_gval = lax.dot_general(
        dense_gate, full_rows, contract_last, preferred_element_type=jnp.float32
    )
    dense_uval = lax.dot_general(
        dense_up, full_rows, contract_last, preferred_element_type=jnp.float32
    )
    dense_hidden = (jax.nn.silu(dense_gval) * dense_uval).astype(jnp.bfloat16)
    dense_part = lax.psum_scatter(
        lax.dot_general(
            dense_down, dense_hidden, (((0,), (0,)), ((), ())), preferred_element_type=jnp.float32
        ).astype(jnp.bfloat16),
        "tp",
        scatter_dimension=0,
        tiled=True,
    ).astype(jnp.float32)
    mixed = mixture + jax.nn.sigmoid(branch_gate)[None, :] * jnp.transpose(dense_part)
    return mixed.astype(jnp.bfloat16)


def solution(mesh):
    in_specs = (
        P("ep", "tp"),
        P("ep", None, None),
        P("ep", None, None),
        P("ep", "tp", None),
        P("ep", "tp", None),
        P("ep", None, "tp"),
        P("tp", None),
        P("tp", None),
        P("tp", None),
        P("tp"),
    )
    out_specs = P("ep", "tp")
    return jax.shard_map(
        per_device, mesh=mesh, in_specs=in_specs, out_specs=out_specs, check_vma=False
    )
```

profile of v0, /device:TPU:0, one launch (start us, length us, event | category | flops | bytes accessed | tf_op | source)
XLA Modules:
  0.0 113.7 jit_solution(1492164187897772887)
XLA Ops:
  6.5 0.0 copy-start
  6.5 0.0 all-gather.5.cloned.1.call-start
  6.5 0.7 all-gather.5.cloned.1.call-update
  7.3 0.0 all-gather.3.cloned.1.call-start
  7.3 0.8 reshape.54
  8.1 2.1 %gather_fusion = bf16[224,512]{1,0:T(8,128)(2,1)S(1)} fusion(bf16[224,512]{1,0:T(8,128)(2,1)} %param.10, s32[1024]{0:T(1024)S(1)} %pad_clamp_fusion), kind=kCustom, calls=%fused_computation | custom fusion | bytes 459648 | tf_op jit(solution)/shard_map/jit(_take)/gather | solution.py:24
  10.2 0.0 copy-done.3
  10.2 0.1 broadcast_select_fusion
  10.3 10.7 %all_to_all.10 = bf16[4,56,512]{2,1,0:T(8,128)(2,1)} all-to-all(bf16[4,56,512]{2,1,0:T(8,128)(2,1)S(1)} %broadcast_select_fusion), channel_id=1, replica_groups=mesh['ep'=4,'tp'=8] {'ep'}, dimensions={0} | all-to-all | bytes 458752 | tf_op jit(solution)/shard_map/all_to_all | solution.py:25
  21.1 0.0 all-gather.3.cloned.1.call-update
  21.1 0.0 reduce-scatter.2.cloned.1.call-start
  21.1 17.6 %all-gather.5.cloned.1.call-done = bf16[224,4096]{1,0:T(8,128)(2,1)} async-done(((bf16[224,512]{1,0:T(8,128)(2,1)}), bf16[224,4096]{1,0:T(8,128)(2,1)}) %all-gather.5.cloned.1.call-update) | async-done | bytes 1835024 | tf_op jit(solution)/shard_map/all_gather | solution.py:23
  38.7 5.8 %fusion.32 = f32[640,224]{0,1:T(8,128)} fusion(bf16[640,4096]{1,0:T(8,128)(2,1)} %param.16, bf16[224,4096]{1,0:T(8,128)(2,1)} %all-gather.5.cloned.1.call-done), kind=kOutput, calls=%fused_computation.35 | convolution fusion | flops 1174405120 | bytes 7651328 | tf_op jit(solution)/shard_map/dot_general | solution.py:56
  44.6 0.0 copy-done.6
  44.6 10.1 %fusion = bf16[4096,224]{0,1:T(8,128)(2,1)} fusion(bf16[640,4096]{1,0:T(8,128)(2,1)} %param.18, bf16[640,4096]{1,0:T(8,128)(2,1)} %param.17, bf16[224,4096]{1,0:T(8,128)(2,1)S(1)} %copy-done.6, f32[640,224]{0,1:T(8,128)} %fusion.32), kind=kOutput, calls=%fused_computation.2 | convolution fusion | flops 2350587904 | bytes 14729216 | tf_op jit(solution)/shard_map/dot_general | solution.py:64
  54.6 0.0 reduce-scatter.2.cloned.1.call-update
  54.7 0.7 copy-done.5
  55.3 0.1 select_reduce_fusion
  55.5 11.3 %all-gather.3.cloned.1.call-done = bf16[4,56,4096]{2,1,0:T(8,128)(2,1)} async-done(((bf16[4,56,512]{2,1,0:T(8,128)(2,1)}), bf16[4,56,4096]{2,1,0:T(8,128)(2,1)}) %all-gather.3.cloned.1.call-update) | async-done | bytes 1835024 | tf_op jit(solution)/shard_map/all_gather | solution.py:26
  66.8 0.0 copy-done.2
  66.8 2.4 %fusion.11 = f32[160,224]{1,0:T(8,128)S(1)} fusion(bf16[224,4096]{1,0:T(8,128)(2,1)} %bitcast.49, bf16[1,160,4096]{2,1,0:T(8,128)(2,1)S(1)} %copy-done.2), kind=kOutput, calls=%fused_computation.13 | convolution fusion | flops 293601280 | bytes 3289088 | tf_op jit(solution)/shard_map/dot_general | solution.py:29
  69.2 0.0 copy-done.1
  69.2 0.8 fusion.20
  70.0 0.0 copy-start.4
  70.0 17.2 %all_gather.10 = bf16[1280,224]{1,0:T(8,128)(2,1)S(1)} all-gather(bf16[160,224]{1,0:T(8,128)(2,1)S(1)} %fusion.20), channel_id=1, replica_groups=mesh['ep'=4,'tp'=8] {'tp'}, dimensions={0}, use_global_device_ids=true | all-gather | bytes 645120 | tf_op jit(solution)/shard_map/all_gather | solution.py:38
  87.2 0.0 copy-done
  87.2 1.2 %fusion.8 = bf16[224,512]{1,0:T(8,128)(2,1)} fusion(bf16[1280,224]{1,0:T(8,128)(2,1)S(1)} %all_gather.10, bf16[1,1280,512]{2,1,0:T(8,128)(2,1)S(1)} %copy-done), kind=kOutput, calls=%fused_computation.12 | convolution fusion | flops 293715968 | bytes 2113536 | tf_op jit(solution)/shard_map/dot_general | solution.py:37
  88.4 3.6 %all-to-all-start.1 = ((bf16[4,56,512]{2,1,0:T(8,128)(2,1)}), bf16[4,56,512]{2,1,0:T(8,128)(2,1)S(1)}, u32[]{:S(2)}, u32[]{:S(2)}) async-start(bf16[4,56,512]{2,1,0:T(8,128)(2,1)} %bitcast.10), calls=%async_computation.1 | async-start | bytes 458752 | tf_op jit(solution)/shard_map/all_to_all | solution.py:43
  92.0 5.6 %all-to-all-done.1 = bf16[4,56,512]{2,1,0:T(8,128)(2,1)S(1)} async-done(((bf16[4,56,512]{2,1,0:T(8,128)(2,1)}), bf16[4,56,512]{2,1,0:T(8,128)(2,1)S(1)}, u32[]{:S(2)}, u32[]{:S(2)}) %all-to-all-start.1) | async-done | bytes 229408 | tf_op jit(solution)/shard_map/all_to_all | solution.py:43
  97.6 0.7 multiply_reduce_fusion
  98.3 7.2 %reduce-scatter.2.cloned.1.call-done = bf16[512,224]{0,1:T(8,128)(2,1)} async-done(((bf16[4096,224]{0,1:T(8,128)(2,1)}), bf16[512,224]{0,1:T(8,128)(2,1)}) %reduce-scatter.2.cloned.1.call-update) | async-done | bytes 229392 | tf_op jit(solution)/shard_map/reduce_scatter | solution.py:63
  105.5 1.7 %fusion.28 = bf16[224,512]{1,0:T(8,128)(2,1)} fusion(f32[224,512]{1,0:T(8,128)S(1)} %multiply_reduce_fusion, bf16[512,224]{0,1:T(8,128)(2,1)} %reduce-scatter.2.cloned.1.call-done, f32[512]{0:T(512)S(1)} %add_divide_fusion), kind=kLoop, calls=%fused_computation.23 | loop fusion | flops 458752 | bytes 919552 | tf_op jit(solution)/shard_map/convert_element_type | solution.py:72
  (12 shorter events, 0.0 us)
Async XLA Ops:
  6.5 80.6 %copy-start = (bf16[1,1280,512]{2,1,0:T(8,128)(2,1)S(1)}, bf16[1,1280,512]{2,1,0:T(8,128)(2,1)}, u32[]{:S(2)}) copy-start(bf16[1,1280,512]{2,1,0:T(8,128)(2,1)} %param.15) | copy-start | bytes 3932164
  6.5 3.7 %copy-start.3 = (s32[1,4,56]{2,1,0:T(4,128)S(1)}, s32[1,4,56]{2,1,0:T(4,128)}, u32[]{:S(2)}) copy-start(s32[1,4,56]{2,1,0:T(4,128)} %param.11) | copy-start | bytes 2692
  6.5 32.2 %all-gather.5.cloned.1.call-start = ((), (), s32[]{:S(2)}) async-start(), calls=%async_computation.4 | async-start | bytes 2064384 | tf_op jit(solution)/shard_map/all_gather | solution.py:23
  7.3 59.5 %all-gather.3.cloned.1.call-start = ((), (), s32[]{:S(2)}) async-start(), calls=%async_computation.3 | async-start | bytes 2064384 | tf_op jit(solution)/shard_map/all_gather | solution.py:26
  21.1 84.4 %reduce-scatter.2.cloned.1.call-start = ((), (), s32[]{:S(2)}) async-start(), calls=%async_computation.5 | async-start | bytes 2064384 | tf_op jit(solution)/shard_map/reduce_scatter | solution.py:63
  38.7 5.8 %copy-start.6 = (bf16[224,4096]{1,0:T(8,128)(2,1)S(1)}, bf16[224,4096]{1,0:T(8,128)(2,1)}, u32[]{:S(2)}) copy-start(bf16[224,4096]{1,0:T(8,128)(2,1)} %all-gather.5.cloned.1.call-done) | copy-start | bytes 5505028
  54.6 0.7 copy-start.5
  54.6 12.1 %copy-start.2 = (bf16[1,160,4096]{2,1,0:T(8,128)(2,1)S(1)}, bf16[1,160,4096]{2,1,0:T(8,128)(2,1)}, u32[]{:S(2)}) copy-start(bf16[1,160,4096]{2,1,0:T(8,128)(2,1)} %param.13) | copy-start | bytes 3932164
  66.7 2.4 %copy-start.1 = (bf16[4,56,4096]{2,1,0:T(8,128)(2,1)S(1)}, bf16[4,56,4096]{2,1,0:T(8,128)(2,1)}, u32[]{:S(2)}) copy-start(bf16[4,56,4096]{2,1,0:T(8,128)(2,1)} %all-gather.3.cloned.1.call-done) | copy-start | bytes 5505028
  66.8 2.5 %copy-start.7 = (bf16[1,160,4096]{2,1,0:T(8,128)(2,1)S(1)}, bf16[1,160,4096]{2,1,0:T(8,128)(2,1)}, u32[]{:S(2)}) copy-start(bf16[1,160,4096]{2,1,0:T(8,128)(2,1)} %param.14) | copy-start | bytes 3932164
  70.0 22.0 %copy-start.4 = (f32[512]{0:T(512)S(1)}, f32[512]{0:T(512)}, u32[]{:S(2)}) copy-start(f32[512]{0:T(512)} %param.19) | copy-start | bytes 6148
  88.4 9.3 %all-to-all-start.1 = ((bf16[4,56,512]{2,1,0:T(8,128)(2,1)}), bf16[4,56,512]{2,1,0:T(8,128)(2,1)S(1)}, u32[]{:S(2)}, u32[]{:S(2)}) async-start(bf16[4,56,512]{2,1,0:T(8,128)(2,1)} %bitcast.10), calls=%async_computation.1 | async-start | bytes 458752 | tf_op jit(solution)/shard_map/all_to_all | solution.py:43
Sparse Core Ops, SparseCore 0:
  8.9 29.7 all-gather.4
  40.3 26.3 all-gather.2
  69.1 36.3 reduce-scatter.1
where the time goes:
time: 114 us
  waiting for transfers between devices  42.5 us (37%)
  blocking collectives  27.9 us (24%)
  matrix products  21 us (18%)
  between operations  13.2 us (12%)
  starting transfers between devices  3.68 us (3%)
  local copies, waits for them, and re-layouts  3.54 us (3%)
  other arithmetic  1.96 us (2%)
    all_gather x1, waiting for transfers between devices, per_device(): full_rows = lax.all_gather(tokens, 'tp', axis=1, tiled=True)  17.6 us
    all_gather x1, blocking collectives, per_device(): lax.all_gather(hidden, 'tp', axis=0, tiled=True)  17.2 us
    all_gather x1, waiting for transfers between devices, per_device(): arrived = lax.all_gather(landed, 'tp', axis=2, tiled=True)  11.3 us
    all_to_all x1, blocking collectives, per_device(): lax.all_to_all(picked, 'ep', split_axis=0, concat_axis=0, tiled=True)  10.7 us
    dot_general x1, matrix products, per_device(): lax.dot_general(dense_down, dense_hidden, (((0,), (0,)), ((), ())), prefe...  10.1 us
    reduce_scatter x1, waiting for transfers between devices, per_device(): lax.psum_scatter(lax.dot_general(dense_down, dense_hidden, (((0,), (0,)),...  7.2 us
    dot_general x1, matrix products, per_device(): lax.dot_general(dense_gate, full_rows, contract_last, preferred_element_t...  5.83 us
    all_to_all x1, waiting for transfers between devices, per_device(): lax.all_to_all(expert_out.reshape(-1, slots, columns.shape[1]), 'ep', spl...  5.65 us
  transfers between devices with their start and end apart: 4, of which 4 were waited for; matrix products, arithmetic and copies ran while one was open for 21% of the time, Pallas kernels for 0%

commit v1 on v0

v1 whole, which is shorter than its diff:
```python
import functools

import jax
import jax.numpy as jnp
from jax import lax
from jax.experimental import pallas as pl
from jax.experimental.pallas import tpu as pltpu
from jax.sharding import PartitionSpec as P

MESH = pl.DeviceIdType.MESH
BF = jnp.bfloat16
F32 = jnp.float32
CORES = 2
G = 2
NT = (((1,), (1,)), ((), ()))
NN = (((1,), (0,)), ((), ()))


def mm(a, b, dims=NN):
    return lax.dot_general(a, b, dims, preferred_element_type=F32)


def silu(v):
    return v / (1.0 + jnp.exp(-v))


def kernel(
    n_ep, n_tp, pad,
    tok_hbm, pcol, prow, pw, weg_hbm, weu_hbm, wed_hbm, wg_hbm, wu_hbm, wd_hbm, bg,
    out_ref,
    x, wg, wu, wd, weg, weu, wed, acc_g, acc_u, oh, pk, ch, acc_eg, acc_eu,
    hx, acc_o, eo, back, hd, ps, pr, own, ru, rd, su, sd, acc_d,
    w_sem, ag_recv, ag_up, ag_dn, ag_pt, c_recv, c_send, cf_recv, cf_send,
    h_recv, h_send, hf_recv, hf_send, e_recv, e_send, p_recv, p_send,
    ru_recv, ru_send, rd_recv, rd_send,
):
    nz = n_tp // CORES
    rows, dl = x.shape[1], x.shape[2]
    rh = rows // G
    s = lax.axis_index("ep")
    t = lax.axis_index("tp")
    z = t // CORES
    c = t % CORES
    partner = CORES * z + (1 - c)

    loads = [
        pltpu.make_async_copy(src, dst, w_sem.at[i])
        for i, (src, dst) in enumerate(
            [(tok_hbm, x.at[t]), (wg_hbm, wg), (wu_hbm, wu), (weg_hbm, weg),
             (weu_hbm, weu), (wd_hbm, wd), (wed_hbm, wed)]
        )
    ]
    for cp in loads:
        cp.start()

    barrier = pltpu.get_barrier_semaphore()
    pl.semaphore_signal(barrier, inc=1, device_id={"tp": partner}, device_id_type=MESH)
    for k in range(1, nz):
        pl.semaphore_signal(
            barrier, inc=1, device_id={"tp": CORES * ((z + k) % nz) + c}, device_id_type=MESH
        )
    for k in range(1, n_ep):
        pl.semaphore_signal(barrier, inc=1, device_id={"ep": (s + k) % n_ep}, device_id_type=MESH)

    oh[...] = (
        lax.broadcasted_iota(jnp.int32, oh.shape, 1) == pcol[...]
    ).astype(F32).astype(BF)
    acc_g[...] = jnp.zeros_like(acc_g)
    acc_u[...] = jnp.zeros_like(acc_u)
    acc_eg[...] = jnp.zeros_like(acc_eg)
    acc_eu[...] = jnp.zeros_like(acc_eu)
    acc_o[...] = jnp.zeros_like(acc_o)

    def remote(src, dst, ssem, rsem, **dev):
        return pltpu.make_async_remote_copy(
            src_ref=src, dst_ref=dst, send_sem=ssem, recv_sem=rsem,
            device_id=dev, device_id_type=MESH,
        )

    def part(g):
        return pl.ds(g * rh, rh)

    up_dev = jnp.minimum(t + CORES, n_tp - CORES + c)
    dn_dev = jnp.maximum(t - CORES, c)

    def ag_copy(zi, g, ssem, dev):
        j = CORES * zi + c
        ref = x.at[j, part(g), :]
        return remote(ref, ref, ssem.at[zi, g], ag_recv.at[j, g], tp=dev)

    def ag_wait(j, g):
        ref = x.at[j, part(g), :]
        remote(ref, ref, ag_pt.at[0, 0], ag_recv.at[j, g], tp=partner).wait_recv()

    def c_copy(zi, e, src_rows, dst_rows, sem_e, rsem_e):
        j = CORES * zi + c
        return remote(
            pk.at[zi, pl.ds(pl.multiple_of(src_rows, pad), pad), :],
            ch.at[j, pl.ds(pl.multiple_of(dst_rows, pad), pad), :],
            c_send.at[zi, sem_e], c_recv.at[zi, rsem_e], ep=e,
        )

    def cf_copy(zi, core):
        ref = ch.at[CORES * zi + core]
        return remote(ref, ref, cf_send.at[zi], cf_recv.at[zi], tp=partner)

    def cols(j):
        return pl.ds(pl.multiple_of(j * dl, dl), dl)

    def order(i):
        d = (i + 1) // 2
        return z + (1 - 2 * (i % 2)) * d

    steps = 2 * nz - 1

    loads[0].wait()
    pl.semaphore_wait(barrier, 1 + (nz - 1) + (n_ep - 1))

    def forward(zi):
        for g in range(G):
            @pl.when(zi != z)
            def _():
                ag_wait(CORES * zi + c, g)

            @pl.when((zi <= z) & (z < nz - 1))
            def _():
                ag_copy(zi, g, ag_up, up_dev).start()

            @pl.when((zi >= z) & (z > 0))
            def _():
                ag_copy(zi, g, ag_dn, dn_dev).start()

            ag_copy(zi, g, ag_pt, partner).start()

    forward(z)
    loads[1].wait()
    loads[2].wait()

    @pl.loop(0, steps)
    def _(i):
        zi = order(i)

        @pl.when((zi >= 0) & (zi < nz))
        def _():
            @pl.when(zi != z)
            def _():
                forward(zi)

            mine = CORES * zi + c
            pk[zi] = mm(oh[...], x[mine]).astype(BF)
            for k in range(1, n_ep):
                e = (s + k) % n_ep
                c_copy(zi, e, e * pad, s * pad, e, s).start()
            keep = pl.ds(pl.multiple_of(s * pad, pad), pad)
            ch[mine, keep, :] = pk[zi, keep, :]

            @pl.loop(0, CORES)
            def _(q):
                j = CORES * zi + (c + q) % CORES

                @pl.when(q > 0)
                def _():
                    for g in range(G):
                        ag_wait(j, g)

                acc_g[...] += mm(x[j], wg[:, cols(j)], NT)
                acc_u[...] += mm(x[j], wu[:, cols(j)], NT)

    hd[...] = (silu(acc_g[...]) * acc_u[...]).astype(BF)
    loads[5].wait()

    def p_copy(zi):
        return remote(ps.at[zi], pr.at[zi], p_send.at[zi], p_recv.at[zi], tp=partner)

    @pl.loop(0, nz)
    def _(zi):
        ps[zi] = mm(hd[...], wd[:, cols(CORES * zi + (1 - c))]).astype(BF)
        p_copy(zi).start()

    @pl.loop(0, nz)
    def _(zi):
        own[zi] = mm(hd[...], wd[:, cols(CORES * zi + c)]).astype(BF)
        p_copy(zi).wait_recv()
        own[zi] = (own[zi].astype(F32) + pr[zi].astype(F32)).astype(BF)

    def rs_up(zu, g, src):
        return remote(src.at[zu, part(g), :], ru.at[zu, part(g), :],
                      ru_send.at[zu, g], ru_recv.at[zu, g], tp=up_dev)

    def rs_dn(zd, g, src):
        return remote(src.at[zd, part(g), :], rd.at[zd, part(g), :],
                      rd_send.at[zd, g], rd_recv.at[zd, g], tp=dn_dev)

    @pl.when(z == 0)
    def _():
        @pl.loop(0, nz - 1)
        def _(i):
            for g in range(G):
                rs_up(nz - 1 - i, g, own).start()

    @pl.when(z == nz - 1)
    def _():
        @pl.loop(0, nz - 1)
        def _(i):
            for g in range(G):
                rs_dn(i, g, own).start()

    loads[3].wait()
    loads[4].wait()

    @pl.loop(0, steps)
    def _(i):
        zi = order(i)

        @pl.when((zi >= 0) & (zi < nz))
        def _():
            for k in range(1, n_ep):
                e = (s + k) % n_ep
                c_copy(zi, e, e * pad, e * pad, e, e).wait_recv()
            cf_copy(zi, c).start()

            @pl.loop(0, CORES)
            def _(q):
                j = CORES * zi + (c + q) % CORES

                @pl.when(q > 0)
                def _():
                    cf_copy(zi, 1 - c).wait_recv()

                acc_eg[...] += mm(ch[j], weg[:, cols(j)], NT)
                acc_eu[...] += mm(ch[j], weu[:, cols(j)], NT)

    hx[t] = (silu(acc_eg[...]) * acc_eu[...]).astype(BF)

    def h_copy(zo, src_z, sidx):
        ref = hx.at[CORES * src_z + c]
        return remote(ref, ref, h_send.at[sidx], h_recv.at[src_z], tp=CORES * zo + c)

    def hf_copy(zi, core):
        ref = hx.at[CORES * zi + core]
        return remote(ref, ref, hf_send.at[zi], hf_recv.at[zi], tp=partner)

    for k in range(1, nz):
        zo = (z + k) % nz
        h_copy(zo, z, zo).start()
    hf_copy(z, c).start()

    @pl.when((z > 0) & (z < nz - 1))
    def _():
        @pl.loop(0, nz - 1)
        def _(i):
            zu = nz - 1 - i
            zd = i
            for g in range(G):
                @pl.when(zu > z)
                def _():
                    rs_up(zu, g, su).wait_recv()
                    su[zu, part(g), :] = (
                        own[zu, part(g), :].astype(F32) + ru[zu, part(g), :].astype(F32)
                    ).astype(BF)
                    rs_up(zu, g, su).start()

                @pl.when(zd < z)
                def _():
                    rs_dn(zd, g, sd).wait_recv()
                    sd[zd, part(g), :] = (
                        own[zd, part(g), :].astype(F32) + rd[zd, part(g), :].astype(F32)
                    ).astype(BF)
                    rs_dn(zd, g, sd).start()

    loads[6].wait()

    @pl.loop(0, steps)
    def _(i):
        zi = order(i)

        @pl.when((zi >= 0) & (zi < nz))
        def _():
            @pl.when(zi != z)
            def _():
                h_copy((z + 1) % nz, zi, z).wait_recv()
                hf_copy(zi, c).start()

            @pl.loop(0, CORES)
            def _(q):
                j = CORES * zi + (c + q) % CORES

                @pl.when(q > 0)
                def _():
                    hf_copy(zi, 1 - c).wait_recv()

                acc_o[...] += mm(hx[j], wed[j])

    eo[...] = acc_o[...].astype(BF)

    def e_copy(dev, src_i, dst_i, ssem, rsem):
        return remote(
            eo.at[pl.ds(pl.multiple_of(src_i * pad, pad), pad), :],
            back.at[pl.ds(pl.multiple_of(dst_i * pad, pad), pad), :],
            e_send.at[ssem], e_recv.at[rsem], ep=dev,
        )

    for k in range(1, n_ep):
        e = (s + k) % n_ep
        e_copy(e, e, s, e, s).start()
    keep = pl.ds(pl.multiple_of(s * pad, pad), pad)
    back[keep, :] = eo[keep, :]

    acc_d[...] = own[z].astype(F32)

    @pl.when(z > 0)
    def _():
        for g in range(G):
            rs_up(z, g, su).wait_recv()
            acc_d[part(g), :] += ru[z, part(g), :].astype(F32)

    @pl.when(z < nz - 1)
    def _():
        for g in range(G):
            rs_dn(z, g, sd).wait_recv()
            acc_d[part(g), :] += rd[z, part(g), :].astype(F32)

    match = lax.broadcasted_iota(jnp.int32, (rows, prow.shape[1]), 0) == prow[...]
    sel = jnp.where(match, pw[...], 0.0)
    hi = sel.astype(BF)
    lo = (sel - hi.astype(F32)).astype(BF)
    acc_d[...] = acc_d[...] * (1.0 / (1.0 + jnp.exp(-bg[...])))
    for k in range(1, n_ep):
        e = (s + k) % n_ep
        e_copy(e, e, e, e, e).wait_recv()
    out_ref[...] = (acc_d[...] + mm(hi, back[...]) + mm(lo, back[...])).astype(BF)

    @pl.loop(0, nz)
    def _(zi):
        for g in range(G):
            @pl.when((zi <= z) & (z < nz - 1))
            def _():
                ag_copy(zi, g, ag_up, up_dev).wait_send()

            @pl.when((zi >= z) & (z > 0))
            def _():
                ag_copy(zi, g, ag_dn, dn_dev).wait_send()

            ag_copy(zi, g, ag_pt, partner).wait_send()

            @pl.when(zi > z)
            def _():
                rs_up(zi, g, su).wait_send()

            @pl.when(zi < z)
            def _():
                rs_dn(zi, g, sd).wait_send()

        for k in range(1, n_ep):
            e = (s + k) % n_ep
            c_copy(zi, e, e * pad, s * pad, e, s).wait_send()
        cf_copy(zi, c).wait_send()
        p_copy(zi).wait_send()
        hf_copy(zi, c).wait_send()

        @pl.when(zi != z)
        def _():
            h_copy((z + 1) % nz, z, zi).wait_send()

    for k in range(1, n_ep):
        e = (s + k) % n_ep
        e_copy(e, e, s, e, s).wait_send()


def per_device(
    n_ep, n_tp, tokens, picks, pick_weights, gate_weight, up_weight, down_weight,
    dense_gate, dense_up, dense_down, branch_gate,
):
    rows, dl = tokens.shape
    slots = picks.shape[2]
    pad = -(-slots // 16) * 16
    nz = n_tp // CORES
    he, width = gate_weight.shape[1], gate_weight.shape[2]
    hd = dense_gate.shape[0]
    ep_rows = n_ep * pad
    fill = ((0, 0), (0, pad - slots))
    padded = jnp.pad(picks[0], fill, constant_values=-1)
    weights = jnp.pad(pick_weights[0], fill)
    vm = pl.BlockSpec(memory_space=pltpu.VMEM)
    hbm = pl.BlockSpec(memory_space=pl.ANY)
    sem = pltpu.SemaphoreType.DMA
    blocks = pltpu.VMEM((nz, rows, dl), BF)
    return pl.pallas_call(
        functools.partial(kernel, n_ep, n_tp, pad),
        out_shape=jax.ShapeDtypeStruct((rows, dl), BF),
        in_specs=[hbm, vm, vm, vm, hbm, hbm, hbm, hbm, hbm, hbm, vm],
        out_specs=vm,
        scratch_shapes=[
            pltpu.VMEM((n_tp, rows, dl), BF),
            pltpu.VMEM((hd, width), BF),
            pltpu.VMEM((hd, width), BF),
            pltpu.VMEM((hd, width), BF),
            pltpu.VMEM((he, width), BF),
            pltpu.VMEM((he, width), BF),
            pltpu.VMEM((n_tp, he, dl), BF),
            pltpu.VMEM((rows, hd), F32),
            pltpu.VMEM((rows, hd), F32),
            pltpu.VMEM((ep_rows, rows), BF),
            pltpu.VMEM((nz, ep_rows, dl), BF),
            pltpu.VMEM((n_tp, ep_rows, dl), BF),
            pltpu.VMEM((ep_rows, he), F32),
            pltpu.VMEM((ep_rows, he), F32),
            pltpu.VMEM((n_tp, ep_rows, he), BF),
            pltpu.VMEM((ep_rows, dl), F32),
            pltpu.VMEM((ep_rows, dl), BF),
            pltpu.VMEM((ep_rows, dl), BF),
            pltpu.VMEM((rows, hd), BF),
            blocks, blocks, blocks, blocks, blocks, blocks, blocks,
            pltpu.VMEM((rows, dl), F32),
            sem((7,)),
            sem((n_tp, G)), sem((nz, G)), sem((nz, G)), sem((nz, G)),
            sem((nz, n_ep)), sem((nz, n_ep)), sem((nz,)), sem((nz,)),
            sem((nz,)), sem((nz,)), sem((nz,)), sem((nz,)),
            sem((n_ep,)), sem((n_ep,)), sem((nz,)), sem((nz,)),
            sem((nz, G)), sem((nz, G)), sem((nz, G)), sem((nz, G)),
        ],
        compiler_params=pltpu.CompilerParams(
            collective_id=0, has_side_effects=True, vmem_limit_bytes=60 * 1024 * 1024
        ),
    )(
        tokens, padded.reshape(-1, 1), padded.reshape(1, -1), weights.reshape(1, -1),
        gate_weight[0], up_weight[0], down_weight[0].reshape(n_tp, he, dl),
        dense_gate, dense_up, dense_down, branch_gate.reshape(1, -1),
    )


def solution(mesh):
    in_specs = (
        P("ep", "tp"),
        P("ep", None, None),
        P("ep", None, None),
        P("ep", "tp", None),
        P("ep", "tp", None),
        P("ep", None, "tp"),
        P("tp", None),
        P("tp", None),
        P("tp", None),
        P("tp"),
    )
    return jax.shard_map(
        functools.partial(per_device, mesh.shape["ep"], mesh.shape["tp"]),
        mesh=mesh, in_specs=in_specs, out_specs=P("ep", "tp"), check_vma=False,
    )
```

time: 114 us -> 79.5 us (0.70)
  the two profiles are of different devices: /device:TPU:0 before, /device:TPU:13 now
where the time goes in v1:
time: 79.5 us; the launch traced here: 79.3 us
  Pallas kernels  74.3 us (93%)
  local copies, waits for them, and re-layouts  5.05 us (6%)
    pallas_call x1, Pallas kernels, per_device(): pl.pallas_call(functools.partial(kernel, n_ep, n_tp, pad), out_shape=jax....  74.3 us
    unnamed x1, local copies, waits for them, and re-layouts  1.64 us

profile of v1, /device:TPU:13, one launch (start us, length us, event | category | flops | bytes accessed | tf_op | source)
XLA Modules:
  0.0 79.3 jit_solution(6109458075062345203)
XLA Ops:
  0.0 0.7 pad.8
  0.7 0.6 reshape.13.prow
  1.3 0.7 pad.9
  2.0 0.6 reshape.14.pw
  2.6 0.8 %reshape.16.pcol = s32[256,1]{1,0:T(8,128)} reshape(s32[4,64]{1,0:T(4,128)S(1)} %pad.8) | data formatting | bytes 2048 | tf_op jit(solution)/shard_map/reshape | solution.py:426
  3.4 74.3 %shard_map.100 = bf16[224,512]{1,0:T(8,128)(2,1)} custom-call(bf16[224,512]{1,0:T(8,128)(2,1)} %tok_hbm.1, s32[256,1]{1,0:T(8,128)} %reshape.16.pcol, s32[1,256]{1,0:T(1,128)} %reshape.13.prow, f32[1,256]{1,0:T(1,128)} %reshape.14.pw, bf16[160,4096]{1,0:T(8,128)(2,1)} %bitcast.6, bf16[160,4096]{1,0:T(8,128)(2,1)} %bitcast.7, bf16[8,160,512]{2,1,0:T(8,128)(2,1)} %bitcast.8, ...), custom_call_target="tpu_custom_call" | custom-call | tf_op jit(solution)/shard_map/pallas_call | solution.py:388
  77.7 1.6 %copy.13 = bf16[224,512]{1,0:T(8,128)(2,1)} copy(bf16[224,512]{1,0:T(8,128)(2,1)} %shard_map.100) | data formatting | bytes 458752

commit v2 on v1

--- a/solution.py
+++ b/solution.py
@@ -14,6 +14,7 @@
 G = 2
 NT = (((1,), (1,)), ((), ()))
 NN = (((1,), (0,)), ((), ()))
+TN = (((0,), (0,)), ((), ()))
 
 
 def mm(a, b, dims=NN):
@@ -26,7 +27,7 @@
 
 def kernel(
     n_ep, n_tp, pad,
-    tok_hbm, pcol, prow, pw, weg_hbm, weu_hbm, wed_hbm, wg_hbm, wu_hbm, wd_hbm, bg,
+    tok_hbm, pk_in, pw_in, weg_hbm, weu_hbm, wed_hbm, wg_hbm, wu_hbm, wd_hbm, bg,
     out_ref,
     x, wg, wu, wd, weg, weu, wed, acc_g, acc_u, oh, pk, ch, acc_eg, acc_eu,
     hx, acc_o, eo, back, hd, ps, pr, own, ru, rd, su, sd, acc_d,
@@ -62,9 +63,19 @@
     for k in range(1, n_ep):
         pl.semaphore_signal(barrier, inc=1, device_id={"ep": (s + k) % n_ep}, device_id_type=MESH)
 
-    oh[...] = (
-        lax.broadcasted_iota(jnp.int32, oh.shape, 1) == pcol[...]
+    slots = pk_in.shape[2]
+    spread = (
+        lax.broadcasted_iota(jnp.int32, (pad, slots), 0)
+        == lax.broadcasted_iota(jnp.int32, (pad, slots), 1)
     ).astype(F32).astype(BF)
+
+    def match(e):
+        ids = lax.broadcasted_iota(jnp.int32, (rows, slots), 0)
+        return ids == pk_in[0, pl.ds(e, 1), :]
+
+    for e in range(n_ep):
+        hot = match(e).astype(F32).astype(BF)
+        oh[e * pad:(e + 1) * pad, :] = mm(spread, hot, NT).astype(BF)
     acc_g[...] = jnp.zeros_like(acc_g)
     acc_u[...] = jnp.zeros_like(acc_u)
     acc_eg[...] = jnp.zeros_like(acc_eg)
@@ -107,11 +118,12 @@
     def cols(j):
         return pl.ds(pl.multiple_of(j * dl, dl), dl)
 
-    def order(i):
-        d = (i + 1) // 2
-        return z + (1 - 2 * (i % 2)) * d
-
-    steps = 2 * nz - 1
+    near = jnp.minimum(z, nz - 1 - z)
+
+    def order(m):
+        both = z + (1 - 2 * (m % 2)) * ((m + 1) // 2)
+        far = jnp.where(2 * z < nz - 1, z + m - near, z - m + near)
+        return jnp.where(m <= 2 * near, both, far)
 
     loads[0].wait()
     pl.semaphore_wait(barrier, 1 + (nz - 1) + (n_ep - 1))
@@ -133,38 +145,37 @@
             ag_copy(zi, g, ag_pt, partner).start()
 
     forward(z)
-    loads[1].wait()
-    loads[2].wait()
-
-    @pl.loop(0, steps)
-    def _(i):
-        zi = order(i)
-
-        @pl.when((zi >= 0) & (zi < nz))
+
+    def dense_block(j):
+        acc_g[...] += mm(x[j], wg[:, cols(j)], NT)
+        acc_u[...] += mm(x[j], wu[:, cols(j)], NT)
+
+    @pl.loop(0, nz)
+    def _(m):
+        zi = order(m)
+        mine = CORES * zi + c
+        pk[zi] = mm(oh[...], x[mine]).astype(BF)
+        for k in range(1, n_ep):
+            e = (s + k) % n_ep
+            c_copy(zi, e, e * pad, s * pad, e, s).start()
+        keep = pl.ds(pl.multiple_of(s * pad, pad), pad)
+        ch[mine, keep, :] = pk[zi, keep, :]
+
+        @pl.when(m == 0)
         def _():
-            @pl.when(zi != z)
-            def _():
-                forward(zi)
-
-            mine = CORES * zi + c
-            pk[zi] = mm(oh[...], x[mine]).astype(BF)
-            for k in range(1, n_ep):
-                e = (s + k) % n_ep
-                c_copy(zi, e, e * pad, s * pad, e, s).start()
-            keep = pl.ds(pl.multiple_of(s * pad, pad), pad)
-            ch[mine, keep, :] = pk[zi, keep, :]
-
-            @pl.loop(0, CORES)
-            def _(q):
-                j = CORES * zi + (c + q) % CORES
-
-                @pl.when(q > 0)
-                def _():
-                    for g in range(G):
-                        ag_wait(j, g)
-
-                acc_g[...] += mm(x[j], wg[:, cols(j)], NT)
-                acc_u[...] += mm(x[j], wu[:, cols(j)], NT)
+            loads[1].wait()
+            loads[2].wait()
+
+        dense_block(mine)
+
+        @pl.when(m < nz - 1)
+        def _():
+            forward(order(m + 1))
+
+        other = CORES * zi + (1 - c)
+        for g in range(G):
+            ag_wait(other, g)
+        dense_block(other)
 
     hd[...] = (silu(acc_g[...]) * acc_u[...]).astype(BF)
     loads[5].wait()
@@ -208,27 +219,24 @@
     loads[3].wait()
     loads[4].wait()
 
-    @pl.loop(0, steps)
-    def _(i):
-        zi = order(i)
-
-        @pl.when((zi >= 0) & (zi < nz))
-        def _():
-            for k in range(1, n_ep):
-                e = (s + k) % n_ep
-                c_copy(zi, e, e * pad, e * pad, e, e).wait_recv()
-            cf_copy(zi, c).start()
-
-            @pl.loop(0, CORES)
-            def _(q):
-                j = CORES * zi + (c + q) % CORES
-
-                @pl.when(q > 0)
-                def _():
-                    cf_copy(zi, 1 - c).wait_recv()
-
-                acc_eg[...] += mm(ch[j], weg[:, cols(j)], NT)
-                acc_eu[...] += mm(ch[j], weu[:, cols(j)], NT)
+    @pl.loop(0, nz)
+    def _(m):
+        zi = order(m)
+        for k in range(1, n_ep):
+            e = (s + k) % n_ep
+            c_copy(zi, e, e * pad, e * pad, e, e).wait_recv()
+        cf_copy(zi, c).start()
+
+        @pl.loop(0, CORES)
+        def _(q):
+            j = CORES * zi + (c + q) % CORES
+
+            @pl.when(q > 0)
+            def _():
+                cf_copy(zi, 1 - c).wait_recv()
+
+            acc_eg[...] += mm(weg[:, cols(j)], ch[j], NT)
+            acc_eu[...] += mm(weu[:, cols(j)], ch[j], NT)
 
     hx[t] = (silu(acc_eg[...]) * acc_eu[...]).astype(BF)
 
@@ -270,26 +278,23 @@
 
     loads[6].wait()
 
-    @pl.loop(0, steps)
-    def _(i):
-        zi = order(i)
-
-        @pl.when((zi >= 0) & (zi < nz))
+    @pl.loop(0, nz)
+    def _(m):
+        zi = order(m)
+        @pl.when(zi != z)
         def _():
-            @pl.when(zi != z)
-            def _():
-                h_copy((z + 1) % nz, zi, z).wait_recv()
-                hf_copy(zi, c).start()
-
-            @pl.loop(0, CORES)
-            def _(q):
-                j = CORES * zi + (c + q) % CORES
-
-                @pl.when(q > 0)
-                def _():
-                    hf_copy(zi, 1 - c).wait_recv()
-
-                acc_o[...] += mm(hx[j], wed[j])
+            h_copy((z + 1) % nz, zi, z).wait_recv()
+            hf_copy(zi, c).start()
+
+        @pl.loop(0, CORES)
+        def _(q):
+            j = CORES * zi + (c + q) % CORES
+
+            @pl.when(q > 0)
+            def _():
+                hf_copy(zi, 1 - c).wait_recv()
+
+            acc_o[...] += mm(hx[j], wed[j], TN)
 
     eo[...] = acc_o[...].astype(BF)
 
@@ -320,15 +325,17 @@
             rs_dn(z, g, sd).wait_recv()
             acc_d[part(g), :] += rd[z, part(g), :].astype(F32)
 
-    match = lax.broadcasted_iota(jnp.int32, (rows, prow.shape[1]), 0) == prow[...]
-    sel = jnp.where(match, pw[...], 0.0)
-    hi = sel.astype(BF)
-    lo = (sel - hi.astype(F32)).astype(BF)
     acc_d[...] = acc_d[...] * (1.0 / (1.0 + jnp.exp(-bg[...])))
     for k in range(1, n_ep):
         e = (s + k) % n_ep
         e_copy(e, e, e, e, e).wait_recv()
-    out_ref[...] = (acc_d[...] + mm(hi, back[...]) + mm(lo, back[...])).astype(BF)
+    for e in range(n_ep):
+        sel = jnp.where(match(e), pw_in[0, pl.ds(e, 1), :], 0.0)
+        hi = sel.astype(BF)
+        lo = (sel - hi.astype(F32)).astype(BF)
+        got = back[e * pad:(e + 1) * pad, :]
+        acc_d[...] += mm(mm(hi, spread, NT).astype(BF), got) + mm(mm(lo, spread, NT).astype(BF), got)
+    out_ref[...] = acc_d[...].astype(BF)
 
     @pl.loop(0, nz)
     def _(zi):
@@ -378,9 +385,6 @@
     he, width = gate_weight.shape[1], gate_weight.shape[2]
     hd = dense_gate.shape[0]
     ep_rows = n_ep * pad
-    fill = ((0, 0), (0, pad - slots))
-    padded = jnp.pad(picks[0], fill, constant_values=-1)
-    weights = jnp.pad(pick_weights[0], fill)
     vm = pl.BlockSpec(memory_space=pltpu.VMEM)
     hbm = pl.BlockSpec(memory_space=pl.ANY)
     sem = pltpu.SemaphoreType.DMA
@@ -388,7 +392,7 @@
     return pl.pallas_call(
         functools.partial(kernel, n_ep, n_tp, pad),
         out_shape=jax.ShapeDtypeStruct((rows, dl), BF),
-        in_specs=[hbm, vm, vm, vm, hbm, hbm, hbm, hbm, hbm, hbm, vm],
+        in_specs=[hbm, vm, vm, hbm, hbm, hbm, hbm, hbm, hbm, vm],
         out_specs=vm,
         scratch_shapes=[
             pltpu.VMEM((n_tp, rows, dl), BF),
@@ -403,9 +407,9 @@
             pltpu.VMEM((ep_rows, rows), BF),
             pltpu.VMEM((nz, ep_rows, dl), BF),
             pltpu.VMEM((n_tp, ep_rows, dl), BF),
-            pltpu.VMEM((ep_rows, he), F32),
-            pltpu.VMEM((ep_rows, he), F32),
-            pltpu.VMEM((n_tp, ep_rows, he), BF),
+            pltpu.VMEM((he, ep_rows), F32),
+            pltpu.VMEM((he, ep_rows), F32),
+            pltpu.VMEM((n_tp, he, ep_rows), BF),
             pltpu.VMEM((ep_rows, dl), F32),
             pltpu.VMEM((ep_rows, dl), BF),
             pltpu.VMEM((ep_rows, dl), BF),
@@ -423,7 +427,7 @@
             collective_id=0, has_side_effects=True, vmem_limit_bytes=60 * 1024 * 1024
         ),
     )(
-        tokens, padded.reshape(-1, 1), padded.reshape(1, -1), weights.reshape(1, -1),
+        tokens, picks, pick_weights,
         gate_weight[0], up_weight[0], down_weight[0].reshape(n_tp, he, dl),
         dense_gate, dense_up, dense_down, branch_gate.reshape(1, -1),
     )

time: 79.5 us -> 64.4 us (0.81)
  Pallas kernels: 74.3 us -> 62.6 us
  local copies, waits for them, and re-layouts: 5.05 us -> 1.64 us
    pallas_call x1, Pallas kernels: 74.3 us -> 62.6 us  [per_device(): pl.pallas_call(functools.partial(kernel, n_ep, n_tp, pad), out_shape=jax....]
    reshape x3 -> x0, local copies, waits for them, and re-layouts: 2.04 us -> none  [the longest x1 0.79 us: per_device(): padded.reshape(-1, 1)]
    pad x2 -> x0, local copies, waits for them, and re-layouts: 1.37 us -> none  [the longest x1 0.69 us: per_device(): padded = jnp.pad(picks[0], fill, constant_values=-1)]
where the time goes in v2:
time: 64.4 us; the launch traced here: 64.2 us
  Pallas kernels  62.6 us (97%)
  local copies, waits for them, and re-layouts  1.64 us (3%)
    pallas_call x1, Pallas kernels, per_device(): pl.pallas_call(functools.partial(kernel, n_ep, n_tp, pad), out_shape=jax....  62.6 us
    unnamed x1, local copies, waits for them, and re-layouts  1.64 us

profile of v2, /device:TPU:13, one launch (start us, length us, event | category | flops | bytes accessed | tf_op | source)
XLA Modules:
  0.0 64.2 jit_solution(8899165737125490973)
XLA Ops:
  0.0 62.6 %shard_map.100 = bf16[224,512]{1,0:T(8,128)(2,1)} custom-call(bf16[224,512]{1,0:T(8,128)(2,1)} %tok_hbm.1, s32[1,4,56]{2,1,0:T(4,128)} %pk_in.1, f32[1,4,56]{2,1,0:T(4,128)} %pw_in.1, bf16[160,4096]{1,0:T(8,128)(2,1)} %bitcast.4, bf16[160,4096]{1,0:T(8,128)(2,1)} %bitcast.5, bf16[8,160,512]{2,1,0:T(8,128)(2,1)} %bitcast.6, bf16[640,4096]{1,0:T(8,128)(2,1)} %wg_hbm.1, ...), custom_call_target="tpu_custom_call" | custom-call | tf_op jit(solution)/shard_map/pallas_call | solution.py:392
  62.6 1.6 %copy.12 = bf16[224,512]{1,0:T(8,128)(2,1)} copy(bf16[224,512]{1,0:T(8,128)(2,1)} %shard_map.100) | data formatting | bytes 458752
